TPU v7x, 32 devices: a whole 2x2x4 slice. The times are simulated.
32 devices in a mesh: gr: 2 (over x), sp: 8 (over z, y), tp: 2 (over core).
Axes of the slice: x: 2, y: 2, z: 4, core: 2. Of those that a mesh axis runs over, the one named last changes fastest.
Arguments:
- tokens: bfloat16 [8, 1024, 4096], P('gr', 'sp'), parts along dimension 0, may hold values from -6 to 6
- key_weight: bfloat16 [4096, 2048], P('sp', 'tp'), may hold values from -0.09375 to 0.09375
- value_weight: bfloat16 [4096, 2048], P('sp', 'tp'), may hold values from -0.09375 to 0.09375
- log_decay: float32 [32, 8, 1024], P('tp', 'gr', 'sp'), parts along dimension 1, may hold values from -1 to 0, as said below
- new_query: bfloat16 [8, 2048], P('gr', 'tp'), parts along dimension 0, may hold values from -6 to 6
- new_key: bfloat16 [8, 2048], P('gr', 'tp'), parts along dimension 0, may hold values from -24 to 24
- new_value: bfloat16 [8, 2048], P('gr', 'tp'), parts along dimension 0, may hold values from -6 to 6
- step_decay: float32 [32, 8], P('tp', 'gr'), parts along dimension 1, may hold values from -1.5 to -0.05
- norm_gain: float32 [2048], P('tp'), may hold values from 0.1 to 1.9
Outputs:
- state_cache: float32 [512, 32, 64], P('gr', 'tp'), parts along dimension 0
- first_read: bfloat16 [8, 2048], P('gr', 'tp'), parts along dimension 0
There are 2 independent parts, one for each index of `gr`. A program takes and returns all parts, laid end to end along the dimension named above; an argument that names none is the same for every part. Nothing has to cross between parts.
Inputs may be any that keep to these rules, and one draw needn't show every extreme that they name: `log_decay`: every entry is at most zero.
All inputs are finite; a program needn't handle non-finite values.
Results may differ from a plain program's by a relative error of at most 0.0053.
Values may be sent and summed in bfloat16 or wider, within the bound.
A program may use at most 64 MiB of HBM per device.

v0:
```python
import jax
import jax.numpy as jnp
from jax import lax
from jax.sharding import PartitionSpec as P

HEAD_DIM = 64


def entering(x, axis, combine, identity):
    devices, mine = (lax.axis_size(axis), lax.axis_index(axis))
    everything = lax.all_gather(x, axis)
    start = jnp.broadcast_to(jnp.asarray(identity, x.dtype), x.shape)

    def lap(k, before):
        at = devices - 1 - k
        reached = at > mine
        new = combine(before, everything[at])
        return jnp.where(reached, new, before)

    return lax.fori_loop(0, devices, lap, start)


def rotate_half(values, positions):
    half = values.shape[-1] // 2
    inverse = 10000.0 ** (-jnp.arange(half, dtype=jnp.float32) * (2.0 / values.shape[-1]))
    angles = positions[..., None] * inverse
    cosine = jnp.cos(angles)
    sine = jnp.sin(angles)
    first, second = (values[..., :half], values[..., half:])
    return jnp.concatenate(
        [first * cosine - second * sine, second * cosine + first * sine], axis=-1
    )


def add_totals(earlier, later):
    return earlier + later


def shards(
    tokens,
    key_weight,
    value_weight,
    log_decay,
    new_query,
    new_key,
    new_value,
    step_decay,
    norm_gain,
):
    seqs, span, width = tokens.shape
    heads_here = key_weight.shape[1] // HEAD_DIM
    token_rows = tokens.reshape(seqs * span, width)
    whole_keys, whole_values = (
        lax.all_gather(key_weight, "sp", axis=0, tiled=True),
        lax.all_gather(value_weight, "sp", axis=0, tiled=True),
    )
    key_sum = jnp.dot(token_rows, whole_keys, preferred_element_type=jnp.float32)
    value_sum = jnp.dot(token_rows, whole_values, preferred_element_type=jnp.float32)
    key_vectors = (
        lax.optimization_barrier(key_sum.astype(jnp.bfloat16))
        .astype(jnp.float32)
        .reshape(seqs, span, heads_here, HEAD_DIM)
    )
    values = (
        lax.optimization_barrier(value_sum.astype(jnp.bfloat16))
        .astype(jnp.float32)
        .reshape(seqs, span, heads_here, HEAD_DIM)
    )
    devices = lax.axis_size("sp")
    offset = lax.axis_index("sp") * span
    positions = (offset + jnp.arange(span, dtype=jnp.int32)).astype(jnp.float32)
    rkeys = rotate_half(key_vectors, positions[None, :, None]) * HEAD_DIM ** (-0.5)
    totals = jnp.sum(log_decay, axis=-1)
    later_sum = entering(totals, "sp", add_totals, jnp.zeros_like(totals))
    weight = jnp.exp(totals[:, :, None] - jnp.cumsum(log_decay, axis=-1) + later_sum[:, :, None])
    weighted = rkeys * jnp.transpose(weight, (1, 2, 0))[:, :, :, None]
    term = jnp.einsum("stha,sthb->sahb", weighted, values, precision=lax.Precision.HIGHEST)
    term = term.reshape(seqs * HEAD_DIM, heads_here, HEAD_DIM)
    end_pos = jnp.full((seqs, heads_here), float(span * devices), jnp.float32)
    query = rotate_half(new_query.astype(jnp.float32).reshape(seqs, heads_here, HEAD_DIM), end_pos)
    key_new = rotate_half(
        new_key.astype(jnp.float32).reshape(seqs, heads_here, HEAD_DIM), end_pos
    ) * HEAD_DIM ** (-0.5)
    value_new = new_value.astype(jnp.float32).reshape(seqs, heads_here, HEAD_DIM)
    decay_all = jnp.repeat(jnp.exp(step_decay).T, HEAD_DIM, axis=0)
    key_all = jnp.transpose(key_new, (0, 2, 1)).reshape(seqs * HEAD_DIM, heads_here)
    value_all = jnp.repeat(value_new, HEAD_DIM, axis=0)
    summed = lax.psum(term, "sp")
    state_cache = decay_all[:, :, None] * summed + key_all[:, :, None] * value_all
    state_seq = state_cache.reshape(seqs, HEAD_DIM, heads_here, HEAD_DIM)
    raw = jnp.einsum("sha,sahb->shb", query, state_seq, precision=lax.Precision.HIGHEST)
    center = jnp.mean(raw, axis=-1, keepdims=True)
    spread = jnp.mean(jnp.square(raw - center), axis=-1, keepdims=True)
    normed = (raw - center) * lax.rsqrt(spread + 1e-06) * norm_gain.reshape(heads_here, HEAD_DIM)
    first_read = normed.reshape(seqs, heads_here * HEAD_DIM).astype(jnp.bfloat16)
    return (state_cache, first_read)


def solution(mesh):
    placed = (
        P("gr", "sp", None),
        P("sp", "tp"),
        P("sp", "tp"),
        P("tp", "gr", "sp"),
        P("gr", "tp"),
        P("gr", "tp"),
        P("gr", "tp"),
        P("tp", "gr"),
        P("tp"),
    )
    return jax.shard_map(
        shards,
        mesh=mesh,
        in_specs=placed,
        out_specs=(P("gr", "tp", None), P("gr", "tp")),
        check_vma=False,
    )
```

profile of v0, /device:TPU:0, one launch (start us, length us, event | category | flops | bytes accessed | tf_op | source)
XLA Modules:
  0.0 378.3 jit_solution(3645071348651051041)
XLA Ops:
  7.2 0.7 all-gather.7.cloned.1.call-update
  8.0 0.7 all-gather.5.cloned.1.call-update
  9.0 1.1 reduce_window_sum.13
  10.1 28.8 %all-gather.1 = f32[8,16,4]{1,2,0:T(4,128)S(1)} all-gather(f32[1,16,4]{1,2,0:T(4,128)S(1)} %bitcast.52), channel_id=2, replica_groups=mesh['gr'=2,'sp'=8,'tp'=2] {'sp'}, dimensions={0}, use_global_device_ids=true | all-gather | bytes 2304 | tf_op jit(solution)/shard_map/all_gather | solution.py:11
  38.9 0.3 while.16
  39.5 98.0 %all-gather.7.cloned.1.call-done = bf16[4096,1024]{1,0:T(8,128)(2,1)} async-done(((bf16[512,1024]{1,0:T(8,128)(2,1)}), bf16[4096,1024]{1,0:T(8,128)(2,1)}) %all-gather.7.cloned.1.call-update) | async-done | bytes 8388624 | tf_op jit(solution)/shard_map/all_gather | solution.py:54
  137.5 9.1 %convolution_convert_fusion = bf16[512,1024]{1,0:T(8,128)(2,1)S(1)} fusion(bf16[512,4096]{1,0:T(8,128)(2,1)} %bitcast.53, bf16[4096,1024]{1,0:T(8,128)(2,1)} %all-gather.7.cloned.1.call-done), kind=kOutput, calls=%fused_computation.8 | convolution fusion | flops 4295491584 | bytes 13631488 | tf_op jit(solution)/shard_map/dot_general | solution.py:57
  146.6 115.7 %all-gather.5.cloned.1.call-done = bf16[4096,1024]{1,0:T(8,128)(2,1)} async-done(((bf16[512,1024]{1,0:T(8,128)(2,1)}), bf16[4096,1024]{1,0:T(8,128)(2,1)}) %all-gather.5.cloned.1.call-update) | async-done | bytes 8388624 | tf_op jit(solution)/shard_map/all_gather | solution.py:55
  262.3 10.1 %convolution_convert_fusion.1 = bf16[512,1024]{1,0:T(8,128)(2,1)} fusion(bf16[512,4096]{1,0:T(8,128)(2,1)} %bitcast.54, bf16[4096,1024]{1,0:T(8,128)(2,1)} %all-gather.5.cloned.1.call-done), kind=kOutput, calls=%fused_computation.9 | convolution fusion | flops 4295491584 | bytes 13631488 | tf_op jit(solution)/shard_map/dot_general | solution.py:58
  272.4 2.9 reshape.171
  275.4 1.7 copy.30
  277.0 2.9 reshape.158
  279.9 2.1 multiply_subtract_fusion
  282.1 0.6 maximum_multiply_fusion
  282.7 2.1 fusion.5
  284.7 1.4 copy.37
  286.2 2.1 reshape.148
  289.4 1.2 broadcast_in_dim.8
  290.6 1.1 reshape.153
  291.9 73.2 %all-reduce.2.cloned.1.call-done = f32[256,16,64]{0,2,1:T(8,128)} async-done(((f32[256,16,64]{0,2,1:T(8,128)}), f32[256,16,64]{0,2,1:T(8,128)}) %all-reduce.2.cloned.1.call-update) | async-done | bytes 1048592 | tf_op jit(solution)/shard_map/psum | solution.py:88
  365.0 1.4 multiply_add_fusion
  366.4 0.9 reshape.156
  367.3 3.4 fusion.2
  371.1 0.7 convert_element_type.28
  (55 shorter events, 2.2 us)
Async XLA Ops:
  7.2 1.6 copy-start.1
  7.2 130.3 %all-gather.7.cloned.1.call-start = ((), (), s32[]{:S(2)}) async-start(), calls=%async_computation.1 | async-start | bytes 9437184 | tf_op jit(solution)/shard_map/all_gather | solution.py:54
  7.9 254.4 %all-gather.5.cloned.1.call-start = ((), (), s32[]{:S(2)}) async-start(), calls=%async_computation | async-start | bytes 9437184 | tf_op jit(solution)/shard_map/all_gather | solution.py:55
  8.7 356.3 %all-reduce.2.cloned.1.call-start = ((), (), s32[]{:S(2)}) async-start(), calls=%async_computation.2 | async-start | bytes 2097152 | tf_op jit(solution)/shard_map/psum | solution.py:88
  286.2 2.2 copy-start.6
  286.2 2.3 copy-start.5
  286.2 2.5 copy-start.3
  286.2 2.6 copy-start.4
  286.2 3.0 copy-start.2
  366.4 4.3 %copy-start = (f32[256,16,64]{0,2,1:T(8,128)}, f32[256,16,64]{0,2,1:T(8,128)S(1)}, u32[]{:S(2)}) copy-start(f32[256,16,64]{0,2,1:T(8,128)S(1)} %multiply_add_fusion) | copy-start | bytes 3145732
Sparse Core Ops, SparseCore 0:
  10.1 127.3 all-gather.6
  139.6 122.6 all-gather.4
  288.5 76.4 all-reduce.1
where the time goes:
time: 379 us; the launch traced here: 378 us
  waiting for transfers between devices  288 us (76%)
  blocking collectives  28.8 us (8%)
  matrix products  24.7 us (7%)
  local copies, waits for them, and re-layouts  16 us (4%)
  between operations  14 us (4%)
  other arithmetic  6.37 us (2%)
    all_gather x1, waiting for transfers between devices, shards(): lax.all_gather(value_weight, 'sp', axis=0, tiled=True)  116 us
    all_gather x1, waiting for transfers between devices, shards(): lax.all_gather(key_weight, 'sp', axis=0, tiled=True)  98 us
    psum x1, waiting for transfers between devices, shards(): summed = lax.psum(term, 'sp')  73.2 us
    all_gather x1, blocking collectives, entering(): everything = lax.all_gather(x, axis)  28.8 us
    dot_general x1, matrix products, shards(): jnp.dot(token_rows, whole_values, preferred_element_type=jnp.float32)  10.1 us
    dot_general x1, matrix products, shards(): jnp.dot(token_rows, whole_keys, preferred_element_type=jnp.float32)  9.14 us
  transfers between devices with their start and end apart: 3, of which 3 were waited for; matrix products, arithmetic and copies ran while one was open for 4% of the time, Pallas kernels for 0%

commit v1 on v0

--- a/solution.py
+++ b/solution.py
@@ -85,7 +85,7 @@
     decay_all = jnp.repeat(jnp.exp(step_decay).T, HEAD_DIM, axis=0)
     key_all = jnp.transpose(key_new, (0, 2, 1)).reshape(seqs * HEAD_DIM, heads_here)
     value_all = jnp.repeat(value_new, HEAD_DIM, axis=0)
-    summed = lax.psum(term, "sp")
+    summed = jnp.sum(lax.all_gather(term, axis_name="sp"), axis=0)
     state_cache = decay_all[:, :, None] * summed + key_all[:, :, None] * value_all
     state_seq = state_cache.reshape(seqs, HEAD_DIM, heads_here, HEAD_DIM)
     raw = jnp.einsum("sha,sahb->shb", query, state_seq, precision=lax.Precision.HIGHEST)

time: 379 us -> 431 us (1.14)
  waiting for transfers between devices: 288 us -> 333 us
  other arithmetic: 6.37 us -> 12.7 us
    all_gather x0 -> x1, waiting for transfers between devices: none -> 118 us  [shards(): summed = jnp.sum(lax.all_gather(term, axis_name='sp'), axis=0)]
    psum x1 -> x0, waiting for transfers between devices: 73.2 us -> none  [shards(): summed = lax.psum(term, 'sp')]
where the time goes in v1:
time: 431 us
  waiting for transfers between devices  333 us (77%)
  blocking collectives  28.8 us (7%)
  matrix products  24.7 us (6%)
  local copies, waits for them, and re-layouts  17 us (4%)
  between operations  14 us (3%)
  other arithmetic  12.7 us (3%)
    all_gather x1, waiting for transfers between devices, shards(): summed = jnp.sum(lax.all_gather(term, axis_name='sp'), axis=0)  118 us
    all_gather x1, waiting for transfers between devices, shards(): lax.all_gather(value_weight, 'sp', axis=0, tiled=True)  116 us
    all_gather x1, waiting for transfers between devices, shards(): lax.all_gather(key_weight, 'sp', axis=0, tiled=True)  98 us
    all_gather x1, blocking collectives, entering(): everything = lax.all_gather(x, axis)  28.8 us
    dot_general x1, matrix products, shards(): jnp.dot(token_rows, whole_values, preferred_element_type=jnp.float32)  10.1 us
    dot_general x1, matrix products, shards(): jnp.dot(token_rows, whole_keys, preferred_element_type=jnp.float32)  9.14 us
  transfers between devices with their start and end apart: 3, of which 3 were waited for; matrix products, arithmetic and copies ran while one was open for 4% of the time, Pallas kernels for 0%

profile of v1, /device:TPU:0, one launch (start us, length us, event | category | flops | bytes accessed | tf_op | source)
XLA Modules:
  0.0 430.9 jit_solution(15031592654156488314)
XLA Ops:
  7.2 0.7 all-gather.8.cloned.1.call-update
  8.0 0.7 all-gather.6.cloned.1.call-update
  9.0 1.1 reduce_window_sum.13
  10.1 28.8 %all-gather.1 = f32[8,16,4]{1,2,0:T(4,128)S(1)} all-gather(f32[1,16,4]{1,2,0:T(4,128)S(1)} %bitcast.53), channel_id=2, replica_groups=mesh['gr'=2,'sp'=8,'tp'=2] {'sp'}, dimensions={0}, use_global_device_ids=true | all-gather | bytes 2304 | tf_op jit(solution)/shard_map/all_gather | solution.py:11
  39.5 98.0 %all-gather.8.cloned.1.call-done = bf16[4096,1024]{1,0:T(8,128)(2,1)} async-done(((bf16[512,1024]{1,0:T(8,128)(2,1)}), bf16[4096,1024]{1,0:T(8,128)(2,1)}) %all-gather.8.cloned.1.call-update) | async-done | bytes 8388624 | tf_op jit(solution)/shard_map/all_gather | solution.py:54
  137.5 9.1 %convolution_convert_fusion = bf16[512,1024]{1,0:T(8,128)(2,1)S(1)} fusion(bf16[512,4096]{1,0:T(8,128)(2,1)} %bitcast.54, bf16[4096,1024]{1,0:T(8,128)(2,1)} %all-gather.8.cloned.1.call-done), kind=kOutput, calls=%fused_computation.9 | convolution fusion | flops 4295491584 | bytes 13631488 | tf_op jit(solution)/shard_map/dot_general | solution.py:57
  146.6 115.7 %all-gather.6.cloned.1.call-done = bf16[4096,1024]{1,0:T(8,128)(2,1)} async-done(((bf16[512,1024]{1,0:T(8,128)(2,1)}), bf16[4096,1024]{1,0:T(8,128)(2,1)}) %all-gather.6.cloned.1.call-update) | async-done | bytes 8388624 | tf_op jit(solution)/shard_map/all_gather | solution.py:55
  262.3 10.1 %convolution_convert_fusion.1 = bf16[512,1024]{1,0:T(8,128)(2,1)} fusion(bf16[512,4096]{1,0:T(8,128)(2,1)} %bitcast.55, bf16[4096,1024]{1,0:T(8,128)(2,1)} %all-gather.6.cloned.1.call-done), kind=kOutput, calls=%fused_computation.10 | convolution fusion | flops 4295491584 | bytes 13631488 | tf_op jit(solution)/shard_map/dot_general | solution.py:58
  272.4 2.9 reshape.169
  275.4 1.7 copy.34
  277.0 2.9 reshape.156
  279.9 2.1 multiply_subtract_fusion
  282.7 2.1 fusion.5
  284.7 1.4 copy.41
  286.2 2.2 all_gather_reshape.3
  289.5 1.2 broadcast_in_dim.8
  290.8 2.1 reshape.152
  292.9 118.3 %all-gather.10.cloned.1.call-done = f32[8,256,16,64]{1,3,2,0:T(8,128)} async-done(((f32[1,256,16,64]{1,3,2,0:T(8,128)}), f32[8,256,16,64]{1,3,2,0:T(8,128)}) %all-gather.10.cloned.1.call-update) | async-done | bytes 8388624 | tf_op jit(solution)/shard_map/all_gather | solution.py:88
  411.2 4.2 reduce_sum.39
  415.4 0.9 reduce_sum.40
  416.3 2.4 multiply_add_fusion
  418.8 3.4 fusion.2
  422.5 0.7 convert_element_type.28
  423.2 1.2 multiply_add_fusion.1
  (59 shorter events, 3.1 us)
Async XLA Ops:
  7.2 1.6 copy-start.2
  7.2 130.3 %all-gather.8.cloned.1.call-start = ((), (), s32[]{:S(2)}) async-start(), calls=%async_computation.1 | async-start | bytes 9437184 | tf_op jit(solution)/shard_map/all_gather | solution.py:54
  7.9 254.4 %all-gather.6.cloned.1.call-start = ((), (), s32[]{:S(2)}) async-start(), calls=%async_computation | async-start | bytes 9437184 | tf_op jit(solution)/shard_map/all_gather | solution.py:55
  8.7 402.6 %all-gather.10.cloned.1.call-start = ((), (), s32[]{:S(2)}) async-start(), calls=%async_computation.2 | async-start | bytes 9437184 | tf_op jit(solution)/shard_map/all_gather | solution.py:88
  286.1 2.3 copy-start.7
  286.2 2.4 copy-start.6
  286.2 2.6 copy-start.4
  286.2 2.7 copy-start.5
  286.2 3.2 copy-start.3
  289.5 3.4 copy-start
  418.8 4.4 %copy-start.1 = (f32[256,16,64]{0,2,1:T(8,128)S(1)}, f32[256,16,64]{0,2,1:T(8,128)}, u32[]{:S(2)}) copy-start(f32[256,16,64]{0,2,1:T(8,128)} %reshape.152) | copy-start | bytes 3145732
Sparse Core Ops, SparseCore 0:
  10.1 127.3 all-gather.7
  139.6 122.6 all-gather.5
  288.5 122.6 all-gather.9
